TPU v7x, 32 devices: a whole 2x2x4 slice. The times are simulated.
32 devices in a mesh: grp: 2 (over y), fs: 4 (over z), tp: 4 (over x, core).
Axes of the slice: x: 2, y: 2, z: 4, core: 2. Of those that a mesh axis runs over, the one named last changes fastest.
Arguments:
- tokens: bfloat16 [1024, 2048], P(('grp', 'fs'), 'tp'), parts along dimension 0, may hold values from -300 to 300
- routes: int32 [1024, 2], P(('grp', 'fs')), parts along dimension 0, may hold values from 0 to 3, all different within a row; in each aligned block of 128 rows (0 to 127, 128 to 255, ...) at most 128 rows name the same one
- route_scores: float32 [1024, 2], P(('grp', 'fs')), parts along dimension 0, may hold values from 0.05 to 1
- norm_gain: float32 [2048], P('fs'), may hold values from 0.1 to 1.9
- expert_gate: float32 [4, 2048, 256], P(None, 'fs', 'tp'), may hold values from -6 to 6
- expert_up: float32 [4, 2048, 256], P(None, 'fs', 'tp'), may hold values from -6 to 6
- expert_down: float32 [4, 2048, 256], P(None, 'fs', 'tp'), may hold values from -6 to 6
- shared_gate: float32 [2048, 256], P('fs', 'tp'), may hold values from -6 to 6
- shared_up: float32 [2048, 256], P('fs', 'tp'), may hold values from -6 to 6
- shared_down: float32 [2048, 256], P('fs', 'tp'), may hold values from -6 to 6
Outputs:
- served_gate: bfloat16 [8, 2048, 256], P(('grp', 'fs'), 'tp'), parts along dimension 0
- served_up: bfloat16 [8, 2048, 256], P(('grp', 'fs'), 'tp'), parts along dimension 0
- served_down: bfloat16 [8, 2048, 256], P(('grp', 'fs'), 'tp'), parts along dimension 0
- common_gate: bfloat16 [4096, 256], P(('grp', 'tp')), parts along dimension 0
- common_up: bfloat16 [4096, 256], P(('grp', 'tp')), parts along dimension 0
- common_down: bfloat16 [4096, 256], P(('grp', 'tp')), parts along dimension 0
- mixture: bfloat16 [1024, 2048], P(('grp', 'fs'), 'tp'), parts along dimension 0
There are 2 independent parts, one for each index of `grp`. A program takes and returns all parts, laid end to end along the dimension named above; an argument that names none is the same for every part. Nothing has to cross between parts.
Inputs may be any that keep to these rules, and one draw needn't show every extreme that they name: `routes`: each row names 2 different experts. Within the rows of one index of fs (aligned blocks of 128 rows) no expert is named by more than 128 rows, a bound that some block reaches.
All inputs are finite; a program needn't handle non-finite values.
Results may differ from a plain program's by a relative error of at most 0.018.
Values may be sent and summed in bfloat16 or wider, within the bound.
A program may use at most 64 MiB of HBM per device.

v0:
```python
import jax
import jax.numpy as jnp
from jax import lax
from jax.sharding import PartitionSpec as P

D = 2048
H = 256
SH = 256


EPSILON = 1e-05
ROUTED_SCALE = 2.5


def on_device(
    tokens,
    routes,
    route_scores,
    norm_gain,
    expert_gate,
    expert_up,
    expert_down,
    shared_gate,
    shared_up,
    shared_down,
):
    gain_column = norm_gain[:, None]
    gate_rows, up_rows, down_rows = (
        lax.all_to_all(
            (expert_gate * gain_column[None]).astype(jnp.bfloat16),
            "fs",
            split_axis=0,
            concat_axis=1,
            tiled=True,
        ),
        lax.all_to_all(
            (expert_up * gain_column[None]).astype(jnp.bfloat16),
            "fs",
            split_axis=0,
            concat_axis=1,
            tiled=True,
        ),
        lax.all_to_all(
            expert_down.astype(jnp.bfloat16), "fs", split_axis=0, concat_axis=1, tiled=True
        ),
    )
    shared_gate_rows, shared_up_rows, shared_down_rows = (
        lax.all_gather((shared_gate * gain_column).astype(jnp.bfloat16), "fs", axis=0, tiled=True),
        lax.all_gather((shared_up * gain_column).astype(jnp.bfloat16), "fs", axis=0, tiled=True),
        lax.all_gather(shared_down.astype(jnp.bfloat16), "fs", axis=0, tiled=True),
    )
    served_gate, served_up, served_down, common_gate, common_up, common_down = (
        lax.all_to_all(gate_rows[0], "tp", split_axis=0, concat_axis=1, tiled=True),
        lax.all_to_all(up_rows[0], "tp", split_axis=0, concat_axis=1, tiled=True),
        lax.all_to_all(down_rows[0], "tp", split_axis=0, concat_axis=1, tiled=True),
        lax.all_to_all(shared_gate_rows, "tp", split_axis=0, concat_axis=1, tiled=True),
        lax.all_to_all(shared_up_rows, "tp", split_axis=0, concat_axis=1, tiled=True),
        lax.all_to_all(shared_down_rows, "tp", split_axis=0, concat_axis=1, tiled=True),
    )
    values = tokens.astype(jnp.float32)
    feature_sum, square_sum = lax.psum(
        (jnp.sum(values, axis=1), jnp.sum(values * values, axis=1)), "tp"
    )
    average = feature_sum / D
    variance = square_sum / D - average * average
    normed = ((values - average[:, None]) * lax.rsqrt(variance + EPSILON)[:, None]).astype(
        jnp.bfloat16
    )
    shared_gate_part = jnp.dot(normed, common_gate, preferred_element_type=jnp.float32) * D ** (
        -0.5
    )
    shared_up_part = jnp.dot(normed, common_up, preferred_element_type=jnp.float32) * D ** (-0.5)
    shared_gate_total, shared_up_total = (
        lax.psum(shared_gate_part.astype(jnp.bfloat16), "tp").astype(jnp.float32),
        lax.psum(shared_up_part.astype(jnp.bfloat16), "tp").astype(jnp.float32),
    )
    shared_hidden = (jax.nn.silu(shared_gate_total) * shared_up_total).astype(jnp.bfloat16)
    shared_part = jnp.einsum(
        "th,dh->td", shared_hidden, common_down, preferred_element_type=jnp.float32
    ) * SH ** (-0.5)
    tok_rows, top_count = routes.shape
    experts = expert_gate.shape[0]
    capacity = 2 * tok_rows * top_count // experts
    expert_ids = routes.reshape(-1)
    one_hot = (expert_ids[:, None] == jnp.arange(experts, dtype=jnp.int32)[None, :]).astype(
        jnp.int32
    )
    slot_rank = jnp.sum(jnp.cumsum(one_hot, axis=0) * one_hot, axis=1) - 1
    slot_index = expert_ids * capacity + slot_rank
    token_index = jnp.arange(expert_ids.shape[0], dtype=jnp.int32) // top_count
    slot_token = (
        jnp.full((experts * capacity,), tok_rows, jnp.int32).at[slot_index].set(token_index)
    )
    padded = jnp.concatenate([normed, jnp.zeros((1, normed.shape[1]), jnp.bfloat16)], axis=0)
    outgoing = padded[slot_token].reshape(experts, capacity, normed.shape[1])
    received = lax.all_to_all(outgoing, "fs", split_axis=0, concat_axis=0, tiled=True)
    gate_part = jnp.einsum(
        "scd,dh->sch", received, served_gate, preferred_element_type=jnp.float32
    ) * D ** (-0.5)
    up_part = jnp.einsum(
        "scd,dh->sch", received, served_up, preferred_element_type=jnp.float32
    ) * D ** (-0.5)
    gate_total = lax.psum(gate_part.astype(jnp.bfloat16), "tp").astype(jnp.float32)
    up_total = lax.psum(up_part.astype(jnp.bfloat16), "tp").astype(jnp.float32)
    hidden = (jax.nn.silu(gate_total) * up_total).astype(jnp.bfloat16)
    expert_out = jnp.einsum(
        "sch,dh->scd", hidden, served_down, preferred_element_type=jnp.float32
    ) * H ** (-0.5)
    returned = lax.all_to_all(
        expert_out.astype(jnp.bfloat16), "fs", split_axis=0, concat_axis=0, tiled=True
    )
    picked = returned.reshape(experts * capacity, returned.shape[2])[slot_index]
    picked = picked.reshape(tok_rows, top_count, returned.shape[2]).astype(jnp.float32)
    mix_weight = route_scores / jnp.sum(route_scores, axis=1, keepdims=True) * ROUTED_SCALE
    routed_part = jnp.sum(picked * mix_weight[:, :, None], axis=1)
    mixture = (shared_part + routed_part).astype(jnp.bfloat16)
    return (
        served_gate[None],
        served_up[None],
        served_down[None],
        common_gate,
        common_up,
        common_down,
        mixture,
    )


def solution(mesh):
    in_specs = (
        P(("grp", "fs"), "tp"),
        P(("grp", "fs"), None),
        P(("grp", "fs"), None),
        P("fs"),
        P(None, "fs", "tp"),
        P(None, "fs", "tp"),
        P(None, "fs", "tp"),
        P("fs", "tp"),
        P("fs", "tp"),
        P("fs", "tp"),
    )
    out_specs = (
        P(("grp", "fs"), "tp", None),
        P(("grp", "fs"), "tp", None),
        P(("grp", "fs"), "tp", None),
        P(("grp", "tp"), None),
        P(("grp", "tp"), None),
        P(("grp", "tp"), None),
        P(("grp", "fs"), "tp"),
    )
    return jax.shard_map(
        on_device, mesh=mesh, in_specs=in_specs, out_specs=out_specs, check_vma=False
    )
```

profile of v0, /device:TPU:0, one launch (start us, length us, event | category | flops | bytes accessed | tf_op | source)
XLA Modules:
  0.0 194.3 jit_solution(7800079284692387309)
XLA Ops:
  7.2 1.0 multiply_convert_fusion.2
  8.2 15.7 %all_gather.9 = bf16[2048,64]{0,1:T(8,128)(2,1)S(1)} all-gather(bf16[512,64]{0,1:T(8,128)(2,1)S(1)} %get-tuple-element.44), channel_id=1, replica_groups=mesh['grp'=2,'fs'=4,'tp'=4] {'fs'}, dimensions={0}, use_global_device_ids=true | all-gather | bytes 327680 | tf_op jit(solution)/shard_map/all_gather | solution.py:48
  23.8 0.7 copy.112
  24.6 3.5 %all-to-all-start.6 = ((bf16[4,512,64]{1,2,0:T(8,128)(2,1)}), bf16[4,512,64]{1,2,0:T(8,128)(2,1)S(1)}, u32[]{:S(2)}, u32[]{:S(2)}) async-start(bf16[4,512,64]{1,2,0:T(8,128)(2,1)} %bitcast.70), calls=%async_computation.6 | async-start | bytes 524288 | tf_op jit(solution)/shard_map/all_to_all | solution.py:56
  28.5 1.2 reduce-window.6
  30.3 0.1 mul.131
  30.4 14.3 %all_gather.10 = bf16[2048,64]{0,1:T(8,128)(2,1)S(1)} all-gather(bf16[512,64]{0,1:T(8,128)(2,1)S(1)} %get-tuple-element.43), channel_id=1, replica_groups=mesh['grp'=2,'fs'=4,'tp'=4] {'fs'}, dimensions={0}, use_global_device_ids=true | all-gather | bytes 327680 | tf_op jit(solution)/shard_map/all_gather | solution.py:49
  44.8 0.7 copy.111
  45.5 3.4 %all-to-all-start.7 = ((bf16[4,512,64]{1,2,0:T(8,128)(2,1)}), bf16[4,512,64]{1,2,0:T(8,128)(2,1)S(1)}, u32[]{:S(2)}, u32[]{:S(2)}) async-start(bf16[4,512,64]{1,2,0:T(8,128)(2,1)} %bitcast.69), calls=%async_computation.7 | async-start | bytes 524288 | tf_op jit(solution)/shard_map/all_to_all | solution.py:57
  49.0 0.9 multiply_convert_fusion
  49.9 5.0 %all-to-all-done.7 = bf16[4,512,64]{1,2,0:T(8,128)(2,1)S(1)} async-done(((bf16[4,512,64]{1,2,0:T(8,128)(2,1)}), bf16[4,512,64]{1,2,0:T(8,128)(2,1)S(1)}, u32[]{:S(2)}, u32[]{:S(2)}) %all-to-all-start.7) | async-done | bytes 262176 | tf_op jit(solution)/shard_map/all_to_all | solution.py:57
  54.9 5.4 %all-to-all-start = ((bf16[4,512,64]{1,2,0:T(8,128)(2,1)}), bf16[4,512,64]{1,2,0:T(8,128)(2,1)}, u32[]{:S(2)}, u32[]{:S(2)}) async-start(bf16[4,512,64]{1,2,0:T(8,128)(2,1)} %get-tuple-element.46), calls=%async_computation | async-start | bytes 524288 | tf_op jit(solution)/shard_map/all_to_all | solution.py:29
  60.3 8.7 %all-to-all-done = bf16[4,512,64]{1,2,0:T(8,128)(2,1)} async-done(((bf16[4,512,64]{1,2,0:T(8,128)(2,1)}), bf16[4,512,64]{1,2,0:T(8,128)(2,1)}, u32[]{:S(2)}, u32[]{:S(2)}) %all-to-all-start) | async-done | bytes 262176 | tf_op jit(solution)/shard_map/all_to_all | solution.py:29
  69.0 4.2 %all-to-all-start.2 = ((bf16[4,512,64]{1,2,0:T(8,128)(2,1)}), bf16[4,512,64]{1,2,0:T(8,128)(2,1)}, u32[]{:S(2)}, u32[]{:S(2)}) async-start(bf16[4,512,64]{1,2,0:T(8,128)(2,1)} %get-tuple-element.45), calls=%async_computation.2 | async-start | bytes 524288 | tf_op jit(solution)/shard_map/all_to_all | solution.py:36
  73.1 1.4 scatter_custom_fusion
  74.7 6.1 %all-reduce.1 = (f32[128]{0:T(128)S(1)}, f32[128]{0:T(128)S(1)}) all-reduce(f32[128]{0:T(128)S(1)} %get-tuple-element.36, f32[128]{0:T(128)S(1)} %get-tuple-element.35), channel_id=1, replica_groups=mesh['grp'=2,'fs'=4,'tp'=4] {'tp'}, use_global_device_ids=true, to_apply=%region_3.0 | all-reduce | flops 256 | bytes 2048 | tf_op jit(solution)/shard_map/psum | solution.py:61
  80.8 3.4 %all-to-all-start.1 = ((bf16[4,512,64]{1,2,0:T(8,128)(2,1)}), bf16[4,512,64]{1,2,0:T(8,128)(2,1)S(1)}, u32[]{:S(2)}, u32[]{:S(2)}) async-start(bf16[4,512,64]{1,2,0:T(8,128)(2,1)} %all-to-all-done), calls=%async_computation.1 | async-start | bytes 524288 | tf_op jit(solution)/shard_map/all_to_all | solution.py:53
  84.3 5.9 %all-to-all-done.1 = bf16[4,512,64]{1,2,0:T(8,128)(2,1)S(1)} async-done(((bf16[4,512,64]{1,2,0:T(8,128)(2,1)}), bf16[4,512,64]{1,2,0:T(8,128)(2,1)S(1)}, u32[]{:S(2)}, u32[]{:S(2)}) %all-to-all-start.1) | async-done | bytes 262176 | tf_op jit(solution)/shard_map/all_to_all | solution.py:53
  90.1 3.4 %all-to-all-start.3 = ((bf16[4,512,64]{1,2,0:T(8,128)(2,1)}), bf16[4,512,64]{1,2,0:T(8,128)(2,1)S(1)}, u32[]{:S(2)}, u32[]{:S(2)}) async-start(bf16[4,512,64]{1,2,0:T(8,128)(2,1)} %all-to-all-done.2), calls=%async_computation.3 | async-start | bytes 524288 | tf_op jit(solution)/shard_map/all_to_all | solution.py:54
  93.6 2.6 %gather_fusion = bf16[512,512]{1,0:T(8,128)(2,1)} fusion(bf16[129,512]{1,0:T(8,128)(2,1)S(1)} %concatenate.3, s32[1024]{0:T(1024)S(1)} %pad_clamp_fusion.1), kind=kCustom, calls=%fused_computation | custom fusion | bytes 1050624 | tf_op jit(solution)/shard_map/gather | solution.py:95
  96.2 3.3 %all-to-all-done.3 = bf16[4,512,64]{1,2,0:T(8,128)(2,1)S(1)} async-done(((bf16[4,512,64]{1,2,0:T(8,128)(2,1)}), bf16[4,512,64]{1,2,0:T(8,128)(2,1)S(1)}, u32[]{:S(2)}, u32[]{:S(2)}) %all-to-all-start.3) | async-done | bytes 262176 | tf_op jit(solution)/shard_map/all_to_all | solution.py:54
  99.5 4.8 %all-to-all-start.9 = ((bf16[4,128,512]{2,1,0:T(8,128)(2,1)}), bf16[4,128,512]{2,1,0:T(8,128)(2,1)S(1)}, u32[]{:S(2)}, u32[]{:S(2)}) async-start(bf16[4,128,512]{2,1,0:T(8,128)(2,1)} %bitcast.19), calls=%async_computation.9 | async-start | bytes 1048576 | tf_op jit(solution)/shard_map/all_to_all | solution.py:96
  104.3 0.7 convert_element_type.73
  105.0 0.9 fusion.5
  105.9 0.9 fusion.6
  106.7 11.7 %all-to-all-done.9 = bf16[4,128,512]{2,1,0:T(8,128)(2,1)S(1)} async-done(((bf16[4,128,512]{2,1,0:T(8,128)(2,1)}), bf16[4,128,512]{2,1,0:T(8,128)(2,1)S(1)}, u32[]{:S(2)}, u32[]{:S(2)}) %all-to-all-start.9) | async-done | bytes 524320 | tf_op jit(solution)/shard_map/all_to_all | solution.py:96
  118.5 4.0 %all-to-all-start.4 = ((bf16[4,512,64]{1,2,0:T(8,128)(2,1)}), bf16[4,512,64]{1,2,0:T(8,128)(2,1)}, u32[]{:S(2)}, u32[]{:S(2)}) async-start(bf16[4,512,64]{1,2,0:T(8,128)(2,1)} %convert_element_type.73), calls=%async_computation.4 | async-start | bytes 524288 | tf_op jit(solution)/shard_map/all_to_all | solution.py:43
  122.6 1.0 fusion.1
  123.6 1.0 fusion.2
  124.7 6.3 %all-to-all-done.4 = bf16[4,512,64]{1,2,0:T(8,128)(2,1)} async-done(((bf16[4,512,64]{1,2,0:T(8,128)(2,1)}), bf16[4,512,64]{1,2,0:T(8,128)(2,1)}, u32[]{:S(2)}, u32[]{:S(2)}) %all-to-all-start.4) | async-done | bytes 262176 | tf_op jit(solution)/shard_map/all_to_all | solution.py:43
  131.0 3.4 %all-to-all-start.5 = ((bf16[4,512,64]{1,2,0:T(8,128)(2,1)}), bf16[4,512,64]{1,2,0:T(8,128)(2,1)S(1)}, u32[]{:S(2)}, u32[]{:S(2)}) async-start(bf16[4,512,64]{1,2,0:T(8,128)(2,1)} %all-to-all-done.4), calls=%async_computation.5 | async-start | bytes 524288 | tf_op jit(solution)/shard_map/all_to_all | solution.py:55
  134.5 14.0 %all_gather.11 = bf16[2048,64]{0,1:T(8,128)(2,1)S(1)} all-gather(bf16[512,64]{0,1:T(8,128)(2,1)S(1)} %convert_element_type.76), channel_id=1, replica_groups=mesh['grp'=2,'fs'=4,'tp'=4] {'fs'}, dimensions={0}, use_global_device_ids=true | all-gather | bytes 327680 | tf_op jit(solution)/shard_map/all_gather | solution.py:50
  148.5 0.7 copy.110
  149.2 3.4 %all-to-all-start.8 = ((bf16[4,512,64]{1,2,0:T(8,128)(2,1)}), bf16[4,512,64]{1,2,0:T(8,128)(2,1)S(1)}, u32[]{:S(2)}, u32[]{:S(2)}) async-start(bf16[4,512,64]{1,2,0:T(8,128)(2,1)} %bitcast.68), calls=%async_computation.8 | async-start | bytes 524288 | tf_op jit(solution)/shard_map/all_to_all | solution.py:58
  152.6 11.4 %all-reduce.5.cloned.1.call-done = (bf16[4,128,256]{2,1,0:T(8,128)(2,1)}, bf16[4,128,256]{2,1,0:T(8,128)(2,1)}, bf16[128,256]{1,0:T(8,128)(2,1)}, bf16[128,256]{1,0:T(8,128)(2,1)}) async-done(((bf16[4,128,256]{2,1,0:T(8,128)(2,1)}, bf16[4,128,256]{2,1,0:T(8,128)(2,1)}, bf16[128,256]{1,0:T(8,128)(2,1)}, bf16[128,256]{1,0:T(8,128)(2,1)}), (bf16[4,128,256]{2,1,0:T(8,128)(2,1)}, bf16[4,128,256]{2,1,0:T(8,128)(2,1)}, ...) | async-done | bytes 655376 | tf_op jit(solution)/shard_map/psum | solution.py:104
  164.0 2.2 %fusion = bf16[4,128,512]{2,1,0:T(8,128)(2,1)} fusion(bf16[512,256,1]{0,1,2:T(8,128)(2,1)S(1)} %bitcast.85, bf16[4,128,256]{2,1,0:T(8,128)(2,1)} %get-tuple-element.39, bf16[4,128,256]{2,1,0:T(8,128)(2,1)} %get-tuple-element.40), kind=kOutput, calls=%fused_computation.4 | convolution fusion | flops 135790592 | bytes 1310720 | tf_op jit(solution)/shard_map/sch,dh->scd/dot_general | solution.py:106
  166.2 4.4 %all-to-all-start.10 = ((bf16[4,128,512]{2,1,0:T(8,128)(2,1)}), bf16[4,128,512]{2,1,0:T(8,128)(2,1)S(1)}, u32[]{:S(2)}, u32[]{:S(2)}) async-start(bf16[4,128,512]{2,1,0:T(8,128)(2,1)} %fusion), calls=%async_computation.10 | async-start | bytes 1048576 | tf_op jit(solution)/shard_map/all_to_all | solution.py:109
  170.8 0.8 copy.93
  171.6 0.8 copy.94
  172.4 0.8 copy.95
  173.3 0.8 copy.90
  174.1 0.8 copy.91
  175.0 0.8 copy.92
  175.8 8.4 %all-to-all-done.10 = bf16[4,128,512]{2,1,0:T(8,128)(2,1)S(1)} async-done(((bf16[4,128,512]{2,1,0:T(8,128)(2,1)}), bf16[4,128,512]{2,1,0:T(8,128)(2,1)S(1)}, u32[]{:S(2)}, u32[]{:S(2)}) %all-to-all-start.10) | async-done | bytes 524320 | tf_op jit(solution)/shard_map/all_to_all | solution.py:109
  184.2 1.2 gather_fusion.1
  185.4 0.3 reshape.119
  185.8 0.7 multiply_reduce_fusion
  186.6 0.9 fusion.4
  (53 shorter events, 1.6 us)
Async XLA Ops:
  24.6 3.6 %copy-start.6 = (s32[128,2]{0,1:T(2,128)S(1)}, s32[128,2]{0,1:T(2,128)}, u32[]{:S(2)}) copy-start(s32[128,2]{0,1:T(2,128)} %param.11) | copy-start | bytes 3076
  24.6 20.9 %all-to-all-start.6 = ((bf16[4,512,64]{1,2,0:T(8,128)(2,1)}), bf16[4,512,64]{1,2,0:T(8,128)(2,1)S(1)}, u32[]{:S(2)}, u32[]{:S(2)}) async-start(bf16[4,512,64]{1,2,0:T(8,128)(2,1)} %bitcast.70), calls=%async_computation.6 | async-start | bytes 524288 | tf_op jit(solution)/shard_map/all_to_all | solution.py:56
  44.8 4.2 %copy-start.1 = (f32[4,512,64]{1,2,0:T(8,128)S(1)}, f32[4,512,64]{1,2,0:T(8,128)}, u32[]{:S(2)}) copy-start(f32[4,512,64]{1,2,0:T(8,128)} %param.15) | copy-start | bytes 1572868
  44.8 4.2 %copy-start.2 = (f32[4,512,64]{1,2,0:T(8,128)S(1)}, f32[4,512,64]{1,2,0:T(8,128)}, u32[]{:S(2)}) copy-start(f32[4,512,64]{1,2,0:T(8,128)} %param.14) | copy-start | bytes 1572868
  45.5 3.5 %copy-start.5 = (f32[512]{0:T(512)S(1)}, f32[512]{0:T(512)}, u32[]{:S(2)}) copy-start(f32[512]{0:T(512)} %param.13) | copy-start | bytes 6148
  45.5 9.4 %all-to-all-start.7 = ((bf16[4,512,64]{1,2,0:T(8,128)(2,1)}), bf16[4,512,64]{1,2,0:T(8,128)(2,1)S(1)}, u32[]{:S(2)}, u32[]{:S(2)}) async-start(bf16[4,512,64]{1,2,0:T(8,128)(2,1)} %bitcast.69), calls=%async_computation.7 | async-start | bytes 524288 | tf_op jit(solution)/shard_map/all_to_all | solution.py:57
  54.9 14.0 %all-to-all-start = ((bf16[4,512,64]{1,2,0:T(8,128)(2,1)}), bf16[4,512,64]{1,2,0:T(8,128)(2,1)}, u32[]{:S(2)}, u32[]{:S(2)}) async-start(bf16[4,512,64]{1,2,0:T(8,128)(2,1)} %get-tuple-element.46), calls=%async_computation | async-start | bytes 524288 | tf_op jit(solution)/shard_map/all_to_all | solution.py:29
  69.0 5.6 %copy-start.3 = (bf16[128,512]{1,0:T(8,128)(2,1)S(1)}, bf16[128,512]{1,0:T(8,128)(2,1)}, u32[]{:S(2)}) copy-start(bf16[128,512]{1,0:T(8,128)(2,1)} %param.10) | copy-start | bytes 393220
  69.0 11.8 %all-to-all-start.2 = ((bf16[4,512,64]{1,2,0:T(8,128)(2,1)}), bf16[4,512,64]{1,2,0:T(8,128)(2,1)}, u32[]{:S(2)}, u32[]{:S(2)}) async-start(bf16[4,512,64]{1,2,0:T(8,128)(2,1)} %get-tuple-element.45), calls=%async_computation.2 | async-start | bytes 524288 | tf_op jit(solution)/shard_map/all_to_all | solution.py:36
  80.8 9.4 %all-to-all-start.1 = ((bf16[4,512,64]{1,2,0:T(8,128)(2,1)}), bf16[4,512,64]{1,2,0:T(8,128)(2,1)S(1)}, u32[]{:S(2)}, u32[]{:S(2)}) async-start(bf16[4,512,64]{1,2,0:T(8,128)(2,1)} %all-to-all-done), calls=%async_computation.1 | async-start | bytes 524288 | tf_op jit(solution)/shard_map/all_to_all | solution.py:53
  90.1 9.4 %all-to-all-start.3 = ((bf16[4,512,64]{1,2,0:T(8,128)(2,1)}), bf16[4,512,64]{1,2,0:T(8,128)(2,1)S(1)}, u32[]{:S(2)}, u32[]{:S(2)}) async-start(bf16[4,512,64]{1,2,0:T(8,128)(2,1)} %all-to-all-done.2), calls=%async_computation.3 | async-start | bytes 524288 | tf_op jit(solution)/shard_map/all_to_all | solution.py:54
  99.5 4.8 %copy-start = (f32[4,512,64]{1,2,0:T(8,128)S(1)}, f32[4,512,64]{1,2,0:T(8,128)}, u32[]{:S(2)}) copy-start(f32[4,512,64]{1,2,0:T(8,128)} %param.16) | copy-start | bytes 1572868
  99.5 19.0 %all-to-all-start.9 = ((bf16[4,128,512]{2,1,0:T(8,128)(2,1)}), bf16[4,128,512]{2,1,0:T(8,128)(2,1)S(1)}, u32[]{:S(2)}, u32[]{:S(2)}) async-start(bf16[4,128,512]{2,1,0:T(8,128)(2,1)} %bitcast.19), calls=%async_computation.9 | async-start | bytes 1048576 | tf_op jit(solution)/shard_map/all_to_all | solution.py:96
  118.5 12.5 %all-to-all-start.4 = ((bf16[4,512,64]{1,2,0:T(8,128)(2,1)}), bf16[4,512,64]{1,2,0:T(8,128)(2,1)}, u32[]{:S(2)}, u32[]{:S(2)}) async-start(bf16[4,512,64]{1,2,0:T(8,128)(2,1)} %convert_element_type.73), calls=%async_computation.4 | async-start | bytes 524288 | tf_op jit(solution)/shard_map/all_to_all | solution.py:43
  122.5 41.5 %all-reduce.5.cloned.1.call-start = ((), (), s32[]{:S(2)}) async-start(), calls=%async_computation.11 | async-start | bytes 1310720 | tf_op jit(solution)/shard_map/psum | solution.py:104
  124.7 9.8 %copy-start.4 = (f32[512,64]{0,1:T(8,128)S(1)}, f32[512,64]{0,1:T(8,128)}, u32[]{:S(2)}) copy-start(f32[512,64]{0,1:T(8,128)} %param.19) | copy-start | bytes 393220
  131.0 18.2 %all-to-all-start.5 = ((bf16[4,512,64]{1,2,0:T(8,128)(2,1)}), bf16[4,512,64]{1,2,0:T(8,128)(2,1)S(1)}, u32[]{:S(2)}, u32[]{:S(2)}) async-start(bf16[4,512,64]{1,2,0:T(8,128)(2,1)} %all-to-all-done.4), calls=%async_computation.5 | async-start | bytes 524288 | tf_op jit(solution)/shard_map/all_to_all | solution.py:55
  149.2 17.0 %all-to-all-start.8 = ((bf16[4,512,64]{1,2,0:T(8,128)(2,1)}), bf16[4,512,64]{1,2,0:T(8,128)(2,1)S(1)}, u32[]{:S(2)}, u32[]{:S(2)}) async-start(bf16[4,512,64]{1,2,0:T(8,128)(2,1)} %bitcast.68), calls=%async_computation.8 | async-start | bytes 524288 | tf_op jit(solution)/shard_map/all_to_all | solution.py:58
  166.2 4.4 %copy-start.7 = (f32[128,2]{0,1:T(2,128)S(1)}, f32[128,2]{0,1:T(2,128)}, u32[]{:S(2)}) copy-start(f32[128,2]{0,1:T(2,128)} %param.12) | copy-start | bytes 3076
  166.2 18.0 %all-to-all-start.10 = ((bf16[4,128,512]{2,1,0:T(8,128)(2,1)}), bf16[4,128,512]{2,1,0:T(8,128)(2,1)S(1)}, u32[]{:S(2)}, u32[]{:S(2)}) async-start(bf16[4,128,512]{2,1,0:T(8,128)(2,1)} %fusion), calls=%async_computation.10 | async-start | bytes 1048576 | tf_op jit(solution)/shard_map/all_to_all | solution.py:109
  185.7 0.8 copy-start.8
  185.8 0.9 copy-start.9
Sparse Core Ops, SparseCore 0:
  126.5 37.4 all-reduce.4
where the time goes:
time: 195 us; the launch traced here: 194 us
  waiting for transfers between devices  60.8 us (31%)
  blocking collectives  50.1 us (26%)
  starting transfers between devices  43.3 us (22%)
  between operations  14.3 us (7%)
  local copies, waits for them, and re-layouts  14 us (7%)
  matrix products  6.82 us (3%)
  other arithmetic  5.01 us (3%)
    all_gather x1, blocking collectives, on_device(): lax.all_gather((shared_gate * gain_column).astype(jnp.bfloat16), 'fs', ax...  15.7 us
    all_gather x1, blocking collectives, on_device(): lax.all_gather((shared_up * gain_column).astype(jnp.bfloat16), 'fs', axis...  14.3 us
    all_gather x1, blocking collectives, on_device(): lax.all_gather(shared_down.astype(jnp.bfloat16), 'fs', axis=0, tiled=True)  14 us
    all_to_all x1, waiting for transfers between devices, on_device(): lax.all_to_all(outgoing, 'fs', split_axis=0, concat_axis=0, tiled=True)  11.7 us
    psum x1, waiting for transfers between devices, on_device(): up_total = lax.psum(up_part.astype(jnp.bfloat16), 'tp').astype(jnp.float32)  11.4 us
    all_to_all x1, waiting for transfers between devices, on_device(): lax.all_to_all((expert_gate * gain_column[None]).astype(jnp.bfloat16), 'f...  8.67 us
    all_to_all x1, waiting for transfers between devices, on_device(): lax.all_to_all(expert_out.astype(jnp.bfloat16), 'fs', split_axis=0, conca...  8.45 us
    all_to_all x1, waiting for transfers between devices, on_device(): lax.all_to_all(expert_down.astype(jnp.bfloat16), 'fs', split_axis=0, conc...  6.33 us
  transfers between devices with their start and end apart: 12, of which 8 were waited for; matrix products, arithmetic and copies ran while one was open for 11% of the time, Pallas kernels for 0%

commit v1 on v0

--- a/solution.py
+++ b/solution.py
@@ -1,18 +1,21 @@
+import functools
+
 import jax
 import jax.numpy as jnp
 from jax import lax
+from jax.experimental import pallas as pl
+from jax.experimental.pallas import tpu as pltpu
 from jax.sharding import PartitionSpec as P
 
-D = 2048
-H = 256
-SH = 256
-
-
+LANES = 128
 EPSILON = 1e-05
 ROUTED_SCALE = 2.5
 
 
 def on_device(
+    model_width,
+    hidden_units,
+    shared_units,
     tokens,
     routes,
     route_scores,
@@ -24,6 +27,7 @@
     shared_up,
     shared_down,
 ):
+    D, H, SH = model_width, hidden_units, shared_units
     gain_column = norm_gain[:, None]
     gate_rows, up_rows, down_rows = (
         lax.all_to_all(
@@ -125,6 +129,325 @@
     )
 
 
+def fused_kernel(
+    G, F, T, D, H,
+    tok, routes, scores, gain, eg, eu, ed, sg, su, sd,
+    o_sg, o_su, o_sd, o_cg, o_cu, o_cd, o_mix,
+    w32, sendg, sendd, zg, zd, xg, xd, wfull, dfull,
+    stat, tbuf, pbuf, rbuf, hbuf, obuf, ret,
+    l_sem, zg_s, zg_r, zd_s, zd_r, xg_s, xg_r, xd_s, xd_r,
+    st_s, st_r, tk_s, tk_r, rs_s, rs_r, ag_s, ag_r, rt_s, rt_r, out_sem,
+):
+    y, z, t = lax.axis_index("grp"), lax.axis_index("fs"), lax.axis_index("tp")
+    E, Dz, Hs = eg.shape
+    R, FD = tok.shape
+    hr = Dz // G
+    hd = hr // 2
+    sr = R // T
+
+    def at(y2, z2, t2):
+        return {"grp": y2, "fs": z2, "tp": t2}
+
+    def rc(src, dst, ss, rs, dev):
+        return pltpu.make_async_remote_copy(
+            src_ref=src, dst_ref=dst, send_sem=ss, recv_sem=rs,
+            device_id=dev, device_id_type=pl.DeviceIdType.MESH,
+        )
+
+    half = pl.ds(pl.multiple_of(y * hr, hr), hr)
+    loads = []
+    for i, (ref, sref) in enumerate(((eg, sg), (eu, su), (ed, sd))):
+        loads.append(pltpu.make_async_copy(ref.at[:, half, :], w32.at[i, pl.ds(0, E)], l_sem.at[2 * i]))
+        loads.append(pltpu.make_async_copy(sref.at[half, :], w32.at[i, E], l_sem.at[2 * i + 1]))
+    for c in loads:
+        c.start()
+
+    barrier = pltpu.get_barrier_semaphore()
+    peers = [at(y, lax.rem(z + d, F), t) for d in range(1, F)]
+    for dy in range(G):
+        for dt in range(T):
+            if dy or dt:
+                peers.append(at(lax.rem(y + dy, G), z, lax.rem(t + dt, T)))
+    for dev in peers:
+        pl.semaphore_signal(barrier, inc=1, device_id=dev, device_id_type=pl.DeviceIdType.MESH)
+
+    x = tok[...].astype(jnp.float32)
+    s1 = jnp.sum(x, axis=1, keepdims=True)
+    s2 = jnp.sum(x * x, axis=1, keepdims=True)
+    lane = lax.broadcasted_iota(jnp.int32, (R, LANES), 1)
+    stat[t] = jnp.where(lane == 0, s1, jnp.where(lane == 1, s2, 0.0)).T[0:8]
+    gcol = jnp.concatenate(
+        [
+            jnp.broadcast_to(
+                gain[0:1, pl.ds(pl.multiple_of(y * hr + i * LANES, LANES), LANES)], (LANES, LANES)
+            ).T[:, 0:Hs]
+            for i in range(hr // LANES)
+        ],
+        axis=0,
+    )
+
+    pl.semaphore_wait(barrier, len(peers))
+    stat_copies = []
+    for d in range(1, T):
+        c = rc(stat.at[t], stat.at[t], st_s.at[d - 1], st_r.at[t], at(y, z, lax.rem(t + d, T)))
+        c.start()
+        stat_copies.append(c)
+
+    for c in loads[:4]:
+        c.wait()
+
+    def pack_gu(e):
+        return jnp.concatenate([w32[0, e] * gcol, w32[1, e] * gcol], axis=1).astype(jnp.bfloat16)
+
+    def pack_d(e):
+        return jnp.concatenate([w32[2, e, 0:hd], w32[2, e, hd:hr]], axis=1).astype(jnp.bfloat16)
+
+    common = pack_gu(E)
+    for e in range(E):
+        sendg[e, 0] = pack_gu(e)
+        sendg[e, 1] = common
+    zg_copies = []
+    for d in range(1, F):
+        z2 = lax.rem(z + d, F)
+        c = rc(sendg.at[z2], zg.at[z], zg_s.at[d - 1], zg_r.at[z], at(y, z2, t))
+        c.start()
+        zg_copies.append(c)
+    pltpu.make_async_copy(sendg.at[z], zg.at[z], zg_r.at[z]).start()
+
+    for d in range(1, T):
+        t2 = lax.rem(t + d, T)
+        rc(stat.at[t2], stat.at[t2], st_s.at[d - 1], st_r.at[t2], at(y, z, t2)).wait_recv()
+    tot = stat[0]
+    for i in range(1, T):
+        tot = tot + stat[i]
+    back = jnp.concatenate([tot, jnp.zeros((LANES - 8, R), jnp.float32)], axis=0).T
+    average = back[:, 0:1] / D
+    variance = back[:, 1:2] / D - average * average
+    tbuf[z] = ((tok[...].astype(jnp.float32) - average) * lax.rsqrt(variance + EPSILON)).astype(jnp.bfloat16)
+    tok_copies = []
+    for d in range(1, F):
+        c = rc(tbuf.at[z], tbuf.at[z], tk_s.at[d - 1], tk_r.at[z], at(y, lax.rem(z + d, F), t))
+        c.start()
+        tok_copies.append(c)
+
+    for c in loads[4:]:
+        c.wait()
+    common_d = pack_d(E)
+    for e in range(E):
+        sendd[e, 0] = pack_d(e)
+        sendd[e, 1] = common_d
+    zd_copies = []
+    for d in range(1, F):
+        z2 = lax.rem(z + d, F)
+        c = rc(sendd.at[z2], zd.at[z], zd_s.at[d - 1], zd_r.at[z], at(y, z2, t))
+        c.start()
+        zd_copies.append(c)
+    pltpu.make_async_copy(sendd.at[z], zd.at[z], zd_r.at[z]).start()
+
+    def forward(zb, xb, zr, xs, xr):
+        waits = []
+        for d in range(F):
+            f = lax.rem(z + F - d, F)
+            pltpu.make_async_copy(zb.at[f], zb.at[f], zr.at[f]).wait()
+            for dy in range(G):
+                c = rc(
+                    zb.at[f], xb.at[y * T + t], xs.at[d * G + dy], xr.at[y * T + t],
+                    at(lax.rem(y + dy, G), z, f),
+                )
+                if dy:
+                    c.start()
+                    waits.append((None, c))
+                else:
+                    other = f != t
+                    pl.when(other)(c.start)
+                    own = pltpu.make_async_copy(zb.at[f], xb.at[y * T + t], xr.at[y * T + t])
+                    pl.when(f == t)(own.start)
+                    waits.append((other, c))
+        return waits
+
+    def arrived(xb, xr):
+        for s in range(G * T):
+            pltpu.make_async_copy(xb.at[s], xb.at[s], xr.at[s]).wait()
+
+    xg_waits = forward(zg, xg, zg_r, xg_s, xg_r)
+    arrived(xg, xg_r)
+
+    for k in range(2):
+        for ys in range(G):
+            for p in range(T // 2):
+                a, b = xg[ys * T + 2 * p, k], xg[ys * T + 2 * p + 1, k]
+                rows, cols = pl.ds(ys * hr, hr), pl.ds(p * LANES, LANES)
+                wfull[k, rows, cols] = jnp.concatenate([a[:, :Hs], b[:, :Hs]], axis=1)
+                wfull[k, rows, pl.ds(H + p * LANES, LANES)] = jnp.concatenate([a[:, Hs:], b[:, Hs:]], axis=1)
+    outs = [
+        pltpu.make_async_copy(wfull.at[0, :, pl.ds(0, H)], o_sg, out_sem.at[0]),
+        pltpu.make_async_copy(wfull.at[0, :, pl.ds(H, H)], o_su, out_sem.at[1]),
+        pltpu.make_async_copy(wfull.at[1, :, pl.ds(0, H)], o_cg, out_sem.at[2]),
+        pltpu.make_async_copy(wfull.at[1, :, pl.ds(H, H)], o_cu, out_sem.at[3]),
+    ]
+    for c in outs:
+        c.start()
+
+    spart = (jnp.dot(tbuf[z], wfull[1], preferred_element_type=jnp.float32) * D ** (-0.5)).astype(jnp.bfloat16)
+    for j in range(T):
+        pbuf[j, R:R + sr] = spart[j * sr:(j + 1) * sr]
+    for d in range(1, F):
+        z2 = lax.rem(z + d, F)
+        pltpu.make_async_copy(tbuf.at[z2], tbuf.at[z2], tk_r.at[z2]).wait()
+    rs_copies = []
+    for d in range(T):
+        j = lax.rem(t + 1 + d, T)
+        pbuf[j, 0:R] = (
+            jnp.dot(tbuf[j], wfull[0], preferred_element_type=jnp.float32) * D ** (-0.5)
+        ).astype(jnp.bfloat16)
+        if d < T - 1:
+            c = rc(pbuf.at[j], rbuf.at[t], rs_s.at[d], rs_r.at[t], at(y, z, j))
+            c.start()
+            rs_copies.append(c)
+
+    xd_waits = forward(zd, xd, zd_r, xd_s, xd_r)
+
+    acc = pbuf[t].astype(jnp.float32)
+    for d in range(1, T):
+        t2 = lax.rem(t + d, T)
+        pltpu.make_async_copy(rbuf.at[t2], rbuf.at[t2], rs_r.at[t2]).wait()
+        acc = acc + rbuf[t2].astype(jnp.float32)
+    gate, up = acc[:, 0:H], acc[:, H:]
+    hbuf[t] = (gate / (1.0 + jnp.exp(-gate)) * up).astype(jnp.bfloat16)
+    ag_copies = []
+    for d in range(1, T):
+        c = rc(hbuf.at[t], hbuf.at[t], ag_s.at[d - 1], ag_r.at[t], at(y, z, lax.rem(t + d, T)))
+        c.start()
+        ag_copies.append(c)
+
+    arrived(xd, xd_r)
+    for k in range(2):
+        for ys in range(G):
+            for p in range(T // 2):
+                a, b = xd[ys * T + 2 * p, k], xd[ys * T + 2 * p + 1, k]
+                cols = pl.ds(p * LANES, LANES)
+                dfull[k, pl.ds(ys * hr, hd), cols] = jnp.concatenate([a[:, :Hs], b[:, :Hs]], axis=1)
+                dfull[k, pl.ds(ys * hr + hd, hd), cols] = jnp.concatenate([a[:, Hs:], b[:, Hs:]], axis=1)
+    douts = [
+        pltpu.make_async_copy(dfull.at[0], o_sd, out_sem.at[4]),
+        pltpu.make_async_copy(dfull.at[1], o_cd, out_sem.at[5]),
+    ]
+    for c in douts:
+        c.start()
+    for d in range(1, T):
+        t2 = lax.rem(t + d, T)
+        pltpu.make_async_copy(hbuf.at[t2], hbuf.at[t2], ag_r.at[t2]).wait()
+
+    def down(h, k):
+        return lax.dot_general(
+            h, dfull[k], (((1,), (1,)), ((), ())), preferred_element_type=jnp.float32
+        ) * H ** (-0.5)
+
+    rt_copies = []
+    for d in range(1, F + 1):
+        j = lax.rem(z + d, F)
+        value = down(hbuf[j, 0:R], 0).astype(jnp.bfloat16)
+        if d < F:
+            obuf[j] = value
+            c = rc(obuf.at[j], ret.at[z], rt_s.at[d - 1], rt_r.at[z], at(y, j, t))
+            c.start()
+            rt_copies.append(c)
+        else:
+            ret[z] = value
+    total = down(jnp.concatenate([hbuf[j, R:R + sr] for j in range(T)], axis=0), 1)
+    score_sum = jnp.sum(scores[...], axis=1, keepdims=True)
+    K = routes.shape[1]
+    weight = scores[...] / score_sum * ROUTED_SCALE
+    picked = routes[...]
+    for d in range(1, F):
+        z2 = lax.rem(z + d, F)
+        pltpu.make_async_copy(ret.at[z2], ret.at[z2], rt_r.at[z2]).wait()
+    for e in range(E):
+        share = jnp.sum(jnp.where(picked == e, weight, 0.0), axis=1, keepdims=True)
+        total = total + share * ret[e].astype(jnp.float32)
+    o_mix[...] = total.astype(jnp.bfloat16)
+
+    for c in stat_copies + zg_copies + tok_copies + zd_copies + rs_copies + ag_copies + rt_copies:
+        c.wait_send()
+    for other, c in xg_waits + xd_waits:
+        if other is None:
+            c.wait_send()
+        else:
+            pl.when(other)(c.wait_send)
+    for c in outs + douts:
+        c.wait()
+
+
+def fused(
+    G, F, T,
+    tokens, routes, route_scores, norm_gain,
+    expert_gate, expert_up, expert_down, shared_gate, shared_up, shared_down,
+):
+    R, FD = tokens.shape
+    E, Dz, Hs = expert_gate.shape
+    D, H = FD * T, Hs * T
+    hr = Dz // G
+    hd = hr // 2
+    sr = R // T
+    bf, f32 = jnp.bfloat16, jnp.float32
+    vm, hbm = pl.BlockSpec(memory_space=pltpu.VMEM), pl.BlockSpec(memory_space=pl.ANY)
+    dma = lambda n: pltpu.SemaphoreType.DMA((n,))
+    weights = jax.ShapeDtypeStruct((FD, H), bf)
+    res = pl.pallas_call(
+        functools.partial(fused_kernel, G, F, T, D, H),
+        out_shape=[weights] * 6 + [jax.ShapeDtypeStruct((R, FD), bf)],
+        in_specs=[vm] * 4 + [hbm] * 6,
+        out_specs=[hbm] * 6 + [vm],
+        scratch_shapes=[
+            pltpu.VMEM((3, E + 1, hr, Hs), f32),
+            pltpu.VMEM((E, 2, hr, LANES), bf),
+            pltpu.VMEM((E, 2, hd, LANES), bf),
+            pltpu.VMEM((F, 2, hr, LANES), bf),
+            pltpu.VMEM((F, 2, hd, LANES), bf),
+            pltpu.VMEM((G * T, 2, hr, LANES), bf),
+            pltpu.VMEM((G * T, 2, hd, LANES), bf),
+            pltpu.VMEM((2, FD, 2 * H), bf),
+            pltpu.VMEM((2, FD, H), bf),
+            pltpu.VMEM((T, 8, R), f32),
+            pltpu.VMEM((F, R, FD), bf),
+            pltpu.VMEM((T, R + sr, 2 * H), bf),
+            pltpu.VMEM((T, R + sr, 2 * H), bf),
+            pltpu.VMEM((T, R + sr, H), bf),
+            pltpu.VMEM((F, R, FD), bf),
+            pltpu.VMEM((F, R, FD), bf),
+            dma(6), dma(F), dma(F), dma(F), dma(F),
+            dma(F * G), dma(G * T), dma(F * G), dma(G * T),
+            dma(T), dma(T), dma(F), dma(F), dma(T), dma(T), dma(T), dma(T), dma(F), dma(F), dma(6),
+        ],
+        compiler_params=pltpu.CompilerParams(collective_id=0, has_side_effects=True),
+    )(
+        tokens, routes, route_scores, norm_gain.reshape(1, Dz),
+        expert_gate, expert_up, expert_down, shared_gate, shared_up, shared_down,
+    )
+    return tuple(r[None] for r in res[:3]) + tuple(res[3:])
+
+
+def dispatch(
+    G, F, T,
+    tokens, routes, route_scores, norm_gain,
+    expert_gate, expert_up, expert_down, shared_gate, shared_up, shared_down,
+):
+    R, FD = tokens.shape
+    E, Dz, Hs = expert_gate.shape
+    args = (
+        tokens, routes, route_scores, norm_gain,
+        expert_gate, expert_up, expert_down, shared_gate, shared_up, shared_down,
+    )
+    dense = (
+        F == T and E == F and Dz == FD and 2 * Hs == LANES and R == LANES and T % 2 == 0
+        and shared_gate.shape[1] == Hs and Dz % (2 * LANES * G) == 0 and R % (16 * T) == 0
+        and 2 * R * routes.shape[1] >= E * R
+    )
+    if dense:
+        return fused(G, F, T, *args)
+    return on_device(FD * T, Hs * T, shared_gate.shape[1] * T, *args)
+
+
 def solution(mesh):
     in_specs = (
         P(("grp", "fs"), "tp"),
@@ -148,5 +471,9 @@
         P(("grp", "fs"), "tp"),
     )
     return jax.shard_map(
-        on_device, mesh=mesh, in_specs=in_specs, out_specs=out_specs, check_vma=False
-    )
+        functools.partial(dispatch, mesh.shape["grp"], mesh.shape["fs"], mesh.shape["tp"]),
+        mesh=mesh,
+        in_specs=in_specs,
+        out_specs=out_specs,
+        check_vma=False,
+    )

time: 195 us -> 81.1 us (0.42)
  the two profiles are of different devices: /device:TPU:0 before, /device:TPU:27 now
where the time goes in v1:
time: 81.1 us; the launch traced here: 80.7 us
  Pallas kernels  63.1 us (78%)
  local copies, waits for them, and re-layouts  17 us (21%)
    pallas_call x1, Pallas kernels, fused(): pl.pallas_call(functools.partial(fused_kernel, G, F, T, D, H), out_shape=...  63.1 us
    unnamed x39, local copies, waits for them, and re-layouts  17 us

profile of v1, /device:TPU:27, one launch (start us, length us, event | category | flops | bytes accessed | tf_op | source)
XLA Modules:
  0.0 80.7 jit_solution(9435154031719493544)
XLA Ops:
  0.6 0.0 copy-start.8
  0.6 1.4 %copy.17.routes = s32[128,2]{1,0:T(8,128)} copy(s32[128,2]{0,1:T(2,128)} %param.11) | data formatting | bytes 2048 | tf_op args[1]
  2.1 0.0 copy-start.9
  2.1 1.4 %copy.18.scores = f32[128,2]{1,0:T(8,128)} copy(f32[128,2]{0,1:T(2,128)} %param.12) | data formatting | bytes 2048 | tf_op args[2]
  3.5 0.0 copy-done.8
  3.5 0.0 copy-start
  3.5 0.8 %copy.22.sg = f32[512,64]{1,0:T(8,128)} copy(f32[512,64]{0,1:T(8,128)S(1)} %copy-done.8) | data formatting | bytes 262144 | tf_op args[7]
  4.4 0.0 copy-done.9
  4.4 0.0 copy-start.10
  4.4 0.8 %copy.23.su = f32[512,64]{1,0:T(8,128)} copy(f32[512,64]{0,1:T(8,128)S(1)} %copy-done.9) | data formatting | bytes 262144 | tf_op args[8]
  5.2 0.1 copy-done.10
  5.3 0.8 %copy.24.sd = f32[512,64]{1,0:T(8,128)} copy(f32[512,64]{0,1:T(8,128)S(1)} %copy-done.10) | data formatting | bytes 262144 | tf_op args[9]
  6.1 0.0 copy-done
  6.1 0.0 copy-start.1
  6.1 1.3 %copy.19.eg = f32[4,512,64]{2,1,0:T(8,128)} copy(f32[4,512,64]{1,2,0:T(8,128)S(1)} %copy-done) | data formatting | bytes 1048576 | tf_op args[4]
  7.4 0.0 copy-done.1
  7.4 0.0 copy-start.2
  7.5 1.3 %copy.20.eu = f32[4,512,64]{2,1,0:T(8,128)} copy(f32[4,512,64]{1,2,0:T(8,128)S(1)} %copy-done.1) | data formatting | bytes 1048576 | tf_op args[5]
  8.8 0.0 copy-done.2
  8.8 1.3 %copy.21.ed = f32[4,512,64]{2,1,0:T(8,128)} copy(f32[4,512,64]{1,2,0:T(8,128)S(1)} %copy-done.2) | data formatting | bytes 1048576 | tf_op args[6]
  10.1 63.1 %shard_map.153 = (bf16[512,256]{1,0:T(8,128)(2,1)}, bf16[512,256]{1,0:T(8,128)(2,1)}, bf16[512,256]{1,0:T(8,128)(2,1)}, bf16[512,256]{1,0:T(8,128)(2,1)}, bf16[5...) custom-call(bf16[128,512]{1,0:T(8,128)(2,1)} %tok.1, s32[128,2]{1,0:T(8,128)} %copy.17.routes, ...), custom_call_target="tpu_custom_call" | custom-call | tf_op jit(solution)/shard_map/pallas_call | solution.py:396
  73.2 0.0 copy-start.7
  73.2 1.7 %copy.32 = bf16[1,512,256]{2,1,0:T(8,128)(2,1)} copy(bf16[1,512,256]{2,1,0:T(8,128)(2,1)} %bitcast.6) | data formatting | bytes 524288
  74.9 0.0 copy-done.7
  74.9 0.0 copy-start.6
  74.9 0.7 copy.33
  75.6 0.3 copy-done.6
  76.0 0.0 copy-start.5
  76.0 0.7 copy.34
  76.7 0.3 copy-done.5
  77.0 0.0 copy-start.4
  77.0 0.7 copy.35
  77.7 0.3 copy-done.4
  78.0 0.0 copy-start.3
  78.0 0.7 copy.36
  78.7 0.3 copy-done.3
  79.1 0.0 copy-start.11
  79.1 0.7 copy.37
  79.8 0.3 copy-done.11
  80.1 0.7 copy.38
Async XLA Ops:
  0.6 2.9 %copy-start.8 = (f32[512,64]{0,1:T(8,128)S(1)}, f32[512,64]{0,1:T(8,128)}, u32[]{:S(2)}) copy-start(f32[512,64]{0,1:T(8,128)} %param.17) | copy-start | bytes 393220
  2.1 2.3 %copy-start.9 = (f32[512,64]{0,1:T(8,128)S(1)}, f32[512,64]{0,1:T(8,128)}, u32[]{:S(2)}) copy-start(f32[512,64]{0,1:T(8,128)} %param.18) | copy-start | bytes 393220
  3.5 2.6 %copy-start = (f32[4,512,64]{1,2,0:T(8,128)S(1)}, f32[4,512,64]{1,2,0:T(8,128)}, u32[]{:S(2)}) copy-start(f32[4,512,64]{1,2,0:T(8,128)} %param.14) | copy-start | bytes 1572868
  4.4 0.9 %copy-start.10 = (f32[512,64]{0,1:T(8,128)S(1)}, f32[512,64]{0,1:T(8,128)}, u32[]{:S(2)}) copy-start(f32[512,64]{0,1:T(8,128)} %param.19) | copy-start | bytes 393220
  6.1 1.3 %copy-start.1 = (f32[4,512,64]{1,2,0:T(8,128)S(1)}, f32[4,512,64]{1,2,0:T(8,128)}, u32[]{:S(2)}) copy-start(f32[4,512,64]{1,2,0:T(8,128)} %param.15) | copy-start | bytes 1572868
  7.4 1.3 %copy-start.2 = (f32[4,512,64]{1,2,0:T(8,128)S(1)}, f32[4,512,64]{1,2,0:T(8,128)}, u32[]{:S(2)}) copy-start(f32[4,512,64]{1,2,0:T(8,128)} %param.16) | copy-start | bytes 1572868
  73.2 1.7 %copy-start.7 = (bf16[512,256]{1,0:T(8,128)(2,1)S(1)}, bf16[512,256]{1,0:T(8,128)(2,1)}, u32[]{:S(2)}) copy-start(bf16[512,256]{1,0:T(8,128)(2,1)} %get-tuple-element.15) | copy-start | bytes 786436
  74.9 1.0 %copy-start.6 = (bf16[512,256]{1,0:T(8,128)(2,1)S(1)}, bf16[512,256]{1,0:T(8,128)(2,1)}, u32[]{:S(2)}) copy-start(bf16[512,256]{1,0:T(8,128)(2,1)} %get-tuple-element.16) | copy-start | bytes 786436
  76.0 1.0 %copy-start.5 = (bf16[512,256]{1,0:T(8,128)(2,1)S(1)}, bf16[512,256]{1,0:T(8,128)(2,1)}, u32[]{:S(2)}) copy-start(bf16[512,256]{1,0:T(8,128)(2,1)} %get-tuple-element.31) | copy-start | bytes 786436
  77.0 1.0 %copy-start.4 = (bf16[512,256]{1,0:T(8,128)(2,1)S(1)}, bf16[512,256]{1,0:T(8,128)(2,1)}, u32[]{:S(2)}) copy-start(bf16[512,256]{1,0:T(8,128)(2,1)} %get-tuple-element.32) | copy-start | bytes 786436
  78.0 1.0 %copy-start.3 = (bf16[512,256]{1,0:T(8,128)(2,1)S(1)}, bf16[512,256]{1,0:T(8,128)(2,1)}, u32[]{:S(2)}) copy-start(bf16[512,256]{1,0:T(8,128)(2,1)} %get-tuple-element.33) | copy-start | bytes 786436
  79.1 1.0 %copy-start.11 = (bf16[128,512]{1,0:T(8,128)(2,1)S(1)}, bf16[128,512]{1,0:T(8,128)(2,1)}, u32[]{:S(2)}) copy-start(bf16[128,512]{1,0:T(8,128)(2,1)} %get-tuple-element.34) | copy-start | bytes 393220

commit v2 on v0

--- a/solution.py
+++ b/solution.py
@@ -1,18 +1,21 @@
+import functools
+
 import jax
 import jax.numpy as jnp
 from jax import lax
+from jax.experimental import pallas as pl
+from jax.experimental.pallas import tpu as pltpu
 from jax.sharding import PartitionSpec as P
 
-D = 2048
-H = 256
-SH = 256
-
-
+LANES = 128
 EPSILON = 1e-05
 ROUTED_SCALE = 2.5
 
 
 def on_device(
+    model_width,
+    hidden_units,
+    shared_units,
     tokens,
     routes,
     route_scores,
@@ -24,6 +27,7 @@
     shared_up,
     shared_down,
 ):
+    D, H, SH = model_width, hidden_units, shared_units
     gain_column = norm_gain[:, None]
     gate_rows, up_rows, down_rows = (
         lax.all_to_all(
@@ -125,6 +129,328 @@
     )
 
 
+def fused_kernel(
+    G, F, T, D, H,
+    tok, routes, scores, gain, eg, eu, ed, sg, su, sd,
+    o_sg, o_su, o_sd, o_cg, o_cu, o_cd, o_mix,
+    w32, sendg, sendd, sends, zg, zd, zs, we, de, ws,
+    stat, tbuf, pbuf, rbuf, hbuf, obuf, ret,
+    l_sem, zg_s, zg_r, zd_s, zd_r, zs_s, zs_r, xg_s, xg_r, xd_s, xd_r, xs_s, xs_r,
+    st_s, st_r, tk_s, tk_r, rs_s, rs_r, ag_s, ag_r, rt_s, rt_r,
+):
+    y, z, t = lax.axis_index("grp"), lax.axis_index("fs"), lax.axis_index("tp")
+    E, Hs, Dz = eg.shape
+    R, FD = tok.shape
+    hr = Dz // G
+    sr = R // T
+    bf, f32 = jnp.bfloat16, jnp.float32
+
+    def at(y2, z2, t2):
+        return {"grp": y2, "fs": z2, "tp": t2}
+
+    def rc(src, dst, ss, rs, dev):
+        return pltpu.make_async_remote_copy(
+            src_ref=src, dst_ref=dst, send_sem=ss, recv_sem=rs,
+            device_id=dev, device_id_type=pl.DeviceIdType.MESH,
+        )
+
+    half = pl.ds(pl.multiple_of(y * hr, hr), hr)
+    loads = []
+    for i, (ref, sref) in enumerate(((eg, sg), (eu, su), (ed, sd))):
+        loads.append(pltpu.make_async_copy(ref.at[:, :, half], w32.at[i, pl.ds(0, E)], l_sem.at[2 * i]))
+        loads.append(pltpu.make_async_copy(sref.at[:, half], w32.at[i, E], l_sem.at[2 * i + 1]))
+    loads = [loads[0], loads[2], loads[4], loads[1], loads[3], loads[5]]
+    for c in loads:
+        c.start()
+
+    barrier = pltpu.get_barrier_semaphore()
+    peers = [at(y, lax.rem(z + d, F), t) for d in range(1, F)]
+    for dy in range(G):
+        for dt in range(T):
+            if dy or dt:
+                peers.append(at(lax.rem(y + dy, G), z, lax.rem(t + dt, T)))
+    for dev in peers:
+        pl.semaphore_signal(barrier, inc=1, device_id=dev, device_id_type=pl.DeviceIdType.MESH)
+
+    x = tok[...].astype(f32)
+    s1 = jnp.sum(x, axis=1, keepdims=True)
+    s2 = jnp.sum(x * x, axis=1, keepdims=True)
+    lane = lax.broadcasted_iota(jnp.int32, (R, LANES), 1)
+    stat[t] = jnp.where(lane == 0, s1, jnp.where(lane == 1, s2, 0.0)).T[0:8]
+    gain_row = gain[0:1, half]
+
+    loads[0].wait()
+    loads[1].wait()
+    for e in range(E):
+        sendg[e, 0] = (w32[0, e] * gain_row).astype(bf)
+        sendg[e, 1] = (w32[1, e] * gain_row).astype(bf)
+
+    pl.semaphore_wait(barrier, len(peers))
+    sent = []
+    for d in range(1, T):
+        c = rc(stat.at[t], stat.at[t], st_s.at[d - 1], st_r.at[t], at(y, z, lax.rem(t + d, T)))
+        c.start()
+        sent.append(c)
+
+    def spread(src_of, zb, ss, rr):
+        for d in range(1, F):
+            z2 = lax.rem(z + d, F)
+            c = rc(src_of(z2), zb.at[z], ss.at[d - 1], rr.at[z], at(y, z2, t))
+            c.start()
+            sent.append(c)
+        pltpu.make_async_copy(src_of(z), zb.at[z], rr.at[z]).start()
+
+    spread(lambda e: sendg.at[e], zg, zg_s, zg_r)
+
+    for d in range(1, T):
+        t2 = lax.rem(t + d, T)
+        pltpu.make_async_copy(stat.at[t2], stat.at[t2], st_r.at[t2]).wait()
+    tot = stat[0]
+    for i in range(1, T):
+        tot = tot + stat[i]
+    back = jnp.concatenate([tot, jnp.zeros((LANES - 8, R), f32)], axis=0).T
+    average = back[:, 0:1] / D
+    variance = back[:, 1:2] / D - average * average
+    tbuf[z] = ((tok[...].astype(f32) - average) * lax.rsqrt(variance + EPSILON)).astype(bf)
+    for d in range(1, F):
+        c = rc(tbuf.at[z], tbuf.at[z], tk_s.at[d - 1], tk_r.at[z], at(y, lax.rem(z + d, F), t))
+        c.start()
+        sent.append(c)
+
+    for c in loads[2:]:
+        c.wait()
+    for e in range(E):
+        sendd[e] = w32[2, e].astype(bf)
+    spread(lambda e: sendd.at[e], zd, zd_s, zd_r)
+    sends[0] = (w32[0, E] * gain_row).astype(bf)
+    sends[1] = (w32[1, E] * gain_row).astype(bf)
+    sends[2] = w32[2, E].astype(bf)
+    spread(lambda e: sends, zs, zs_s, zs_r)
+
+    held = []
+
+    def forward(zb, place, zr, xs, xr):
+        for d in range(F):
+            f = lax.rem(z + F - d, F)
+            pltpu.make_async_copy(zb.at[f], zb.at[f], zr.at[f]).wait()
+            for dy in range(G):
+                c = rc(
+                    zb.at[f], place(y, t), xs.at[d * G + dy], xr.at[y * T + t],
+                    at(lax.rem(y + dy, G), z, f),
+                )
+                if dy:
+                    c.start()
+                    sent.append(c)
+                else:
+                    own = pltpu.make_async_copy(zb.at[f], place(y, t), xr.at[y * T + t])
+                    pl.when(f != t)(c.start)
+                    pl.when(f == t)(own.start)
+                    held.append((f != t, c))
+
+    def arrived(place, xr):
+        for ys in range(G):
+            for tt in range(T):
+                pltpu.make_async_copy(place(ys, tt), place(ys, tt), xr.at[ys * T + tt]).wait()
+
+    def columns(ys):
+        return pl.ds(pl.multiple_of(ys * hr, hr), hr)
+
+    def at_e(ys, tt):
+        return we.at[:, tt, :, columns(ys)]
+
+    def at_d(ys, tt):
+        return de.at[tt, :, columns(ys)]
+
+    def at_s(ys, tt):
+        return ws.at[:, tt, :, columns(ys)]
+
+    def rows_of(i):
+        return pl.ds(pl.multiple_of(i * sr, sr), sr)
+
+    def first(s):
+        if 0 < s < F:
+            j = lax.rem(z + F - s, F)
+            pltpu.make_async_copy(tbuf.at[j], tbuf.at[j], tk_r.at[j]).wait()
+        else:
+            j = z
+        w = we[...] if s < F else ws[0:2]
+        pbuf[s] = (
+            lax.dot_general(
+                tbuf[j], w.reshape(2 * H, FD), (((1,), (1,)), ((), ())), preferred_element_type=f32
+            ) * D ** (-0.5)
+        ).astype(bf)
+        for d in range(1, T):
+            t2 = lax.rem(t + d, T)
+            c = rc(pbuf.at[s, rows_of(t2)], rbuf.at[s, t], rs_s.at[s * T + d], rs_r.at[s * T + t], at(y, z, t2))
+            c.start()
+            sent.append(c)
+
+    def second(s):
+        acc = pbuf[s, rows_of(t)].astype(f32)
+        for d in range(1, T):
+            t2 = lax.rem(t + d, T)
+            pltpu.make_async_copy(rbuf.at[s, t2], rbuf.at[s, t2], rs_r.at[s * T + t2]).wait()
+            acc = acc + rbuf[s, t2].astype(f32)
+        gate, up = acc[:, 0:H], acc[:, H:]
+        mine = hbuf.at[s, rows_of(t)]
+        mine[...] = (gate / (1.0 + jnp.exp(-gate)) * up).astype(bf)
+        for d in range(1, T):
+            c = rc(mine, mine, ag_s.at[s * T + d], ag_r.at[s * T + t], at(y, z, lax.rem(t + d, T)))
+            c.start()
+            sent.append(c)
+
+    def third(s):
+        for d in range(1, T):
+            t2 = lax.rem(t + d, T)
+            theirs = hbuf.at[s, rows_of(t2)]
+            pltpu.make_async_copy(theirs, theirs, ag_r.at[s * T + t2]).wait()
+        w = de[...] if s < F else ws[2]
+        value = jnp.dot(hbuf[s], w.reshape(H, FD), preferred_element_type=f32) * H ** (-0.5)
+        if s == F:
+            return value
+        if s == 0:
+            ret[z] = value.astype(bf)
+        else:
+            obuf[s] = value.astype(bf)
+            c = rc(obuf.at[s], ret.at[z], rt_s.at[s], rt_r.at[z], at(y, lax.rem(z + F - s, F), t))
+            c.start()
+            sent.append(c)
+
+    forward(zg, at_e, zg_r, xg_s, xg_r)
+    arrived(at_e, xg_r)
+    first(0)
+    for s in range(1, F):
+        first(s)
+        second(s - 1)
+    second(F - 1)
+    forward(zd, at_d, zd_r, xd_s, xd_r)
+    arrived(at_d, xd_r)
+    for s in range(F):
+        third(s)
+    o_sg[...] = we[0].reshape(H, FD).T
+    o_su[...] = we[1].reshape(H, FD).T
+    o_sd[...] = de[...].reshape(H, FD).T
+    forward(zs, at_s, zs_r, xs_s, xs_r)
+    arrived(at_s, xs_r)
+    first(F)
+    o_cg[...] = ws[0].reshape(H, FD).T
+    second(F)
+    o_cu[...] = ws[1].reshape(H, FD).T
+    o_cd[...] = ws[2].reshape(H, FD).T
+
+    weight = scores[...] / jnp.sum(scores[...], axis=0, keepdims=True) * ROUTED_SCALE
+    picked = routes[...]
+    line = lax.broadcasted_iota(jnp.int32, (LANES, R), 0)
+    shares = jnp.zeros((LANES, R), f32)
+    for e in range(E):
+        share = jnp.sum(jnp.where(picked == e, weight, 0.0), axis=0, keepdims=True)
+        shares = jnp.where(line == e, share, shares)
+    shares = shares.T
+    total = third(F)
+    for d in range(1, F):
+        z2 = lax.rem(z + d, F)
+        pltpu.make_async_copy(ret.at[z2], ret.at[z2], rt_r.at[z2]).wait()
+    for e in range(E):
+        total = total + shares[:, e:e + 1] * ret[e].astype(f32)
+    o_mix[...] = total.astype(bf)
+
+    for c in sent:
+        c.wait_send()
+    for other, c in held:
+        pl.when(other)(c.wait_send)
+
+
+def write_kernel(*refs):
+    count = (len(refs) - 1) // 2
+    sems = refs[-1]
+    copies = [pltpu.make_async_copy(refs[i], refs[count + i], sems.at[i]) for i in range(count)]
+    for c in copies:
+        c.start()
+    for c in copies:
+        c.wait()
+
+
+def fused(
+    G, F, T,
+    tokens, routes, route_scores, norm_gain,
+    expert_gate, expert_up, expert_down, shared_gate, shared_up, shared_down,
+):
+    R, FD = tokens.shape
+    E, Dz, Hs = expert_gate.shape
+    D, H = FD * T, Hs * T
+    hr = Dz // G
+    sr = R // T
+    B = F + 1
+    bf, f32 = jnp.bfloat16, jnp.float32
+    vm, hbm = pl.BlockSpec(memory_space=pltpu.VMEM), pl.BlockSpec(memory_space=pl.ANY)
+    dma = lambda n: pltpu.SemaphoreType.DMA((n,))
+    weights = jax.ShapeDtypeStruct((FD, H), bf)
+    shapes = [weights] * 6 + [jax.ShapeDtypeStruct((R, FD), bf)]
+    res = pl.pallas_call(
+        functools.partial(fused_kernel, G, F, T, D, H),
+        out_shape=shapes,
+        in_specs=[vm] * 4 + [hbm] * 6,
+        out_specs=[vm] * 7,
+        scratch_shapes=[
+            pltpu.VMEM((3, E + 1, Hs, hr), f32),
+            pltpu.VMEM((E, 2, Hs, hr), bf),
+            pltpu.VMEM((E, Hs, hr), bf),
+            pltpu.VMEM((3, Hs, hr), bf),
+            pltpu.VMEM((F, 2, Hs, hr), bf),
+            pltpu.VMEM((F, Hs, hr), bf),
+            pltpu.VMEM((F, 3, Hs, hr), bf),
+            pltpu.VMEM((2, T, Hs, FD), bf),
+            pltpu.VMEM((T, Hs, FD), bf),
+            pltpu.VMEM((3, T, Hs, FD), bf),
+            pltpu.VMEM((T, 8, R), f32),
+            pltpu.VMEM((F, R, FD), bf),
+            pltpu.VMEM((B, R, 2 * H), bf),
+            pltpu.VMEM((B, T, sr, 2 * H), bf),
+            pltpu.VMEM((B, R, H), bf),
+            pltpu.VMEM((F, R, FD), bf),
+            pltpu.VMEM((F, R, FD), bf),
+            dma(6), dma(F), dma(F), dma(F), dma(F), dma(F), dma(F),
+            dma(F * G), dma(G * T), dma(F * G), dma(G * T), dma(F * G), dma(G * T),
+            dma(T), dma(T), dma(F), dma(F),
+            dma(B * T), dma(B * T), dma(B * T), dma(B * T), dma(F), dma(F),
+        ],
+        compiler_params=pltpu.CompilerParams(collective_id=0, has_side_effects=True),
+    )(
+        tokens, routes.T, route_scores.T, norm_gain.reshape(1, Dz),
+        jnp.swapaxes(expert_gate, 1, 2), jnp.swapaxes(expert_up, 1, 2), jnp.swapaxes(expert_down, 1, 2),
+        shared_gate.T, shared_up.T, shared_down.T,
+    )
+    res = pl.pallas_call(
+        write_kernel,
+        out_shape=shapes,
+        in_specs=[vm] * 7,
+        out_specs=[hbm] * 7,
+        scratch_shapes=[dma(7)],
+    )(*res)
+    return tuple(r[None] for r in res[:3]) + tuple(res[3:])
+
+
+def dispatch(
+    G, F, T,
+    tokens, routes, route_scores, norm_gain,
+    expert_gate, expert_up, expert_down, shared_gate, shared_up, shared_down,
+):
+    R, FD = tokens.shape
+    E, Dz, Hs = expert_gate.shape
+    args = (
+        tokens, routes, route_scores, norm_gain,
+        expert_gate, expert_up, expert_down, shared_gate, shared_up, shared_down,
+    )
+    dense = (
+        F == T and E == F and Dz == FD and Hs % 16 == 0 and R == LANES
+        and shared_gate.shape[1] == Hs and Dz % (LANES * G) == 0 and R % (16 * T) == 0
+        and 2 * R * routes.shape[1] >= E * R
+    )
+    if dense:
+        return fused(G, F, T, *args)
+    return on_device(FD * T, Hs * T, shared_gate.shape[1] * T, *args)
+
+
 def solution(mesh):
     in_specs = (
         P(("grp", "fs"), "tp"),
@@ -148,5 +474,9 @@
         P(("grp", "fs"), "tp"),
     )
     return jax.shard_map(
-        on_device, mesh=mesh, in_specs=in_specs, out_specs=out_specs, check_vma=False
-    )
+        functools.partial(dispatch, mesh.shape["grp"], mesh.shape["fs"], mesh.shape["tp"]),
+        mesh=mesh,
+        in_specs=in_specs,
+        out_specs=out_specs,
+        check_vma=False,
+    )

time: 195 us -> 62.2 us (0.32)
  Pallas kernels: 0 us -> 61.1 us
  waiting for transfers between devices: 60.8 us -> 0 us
  blocking collectives: 50.1 us -> 0 us
  starting transfers between devices: 43.3 us -> 0 us
  local copies, waits for them, and re-layouts: 14 us -> 0 us
  between operations: 14.3 us -> 0.64 us
  matrix products: 6.82 us -> 0 us
  other arithmetic: 5.01 us -> 0 us
    pallas_call x0 -> x2, Pallas kernels: none -> 61.1 us  [the longest x1 58.5 us: fused(): pl.pallas_call(functools.partial(fused_kernel, G, F, T, D, H), out_shape=...]
    all_to_all x11 -> x0, waiting for transfers between devices: 49.4 us -> none  [the longest x1 11.7 us: on_device(): lax.all_to_all(outgoing, 'fs', split_axis=0, concat_axis=0, tiled=True)]
    all_gather x3 -> x0, blocking collectives: 44 us -> none  [the longest x1 15.7 us: on_device(): lax.all_gather((shared_gate * gain_column).astype(jnp.bfloat16), 'fs', ax...]
    all_to_all x11 -> x0, starting transfers between devices: 43.3 us -> none  [the longest x1 5.35 us: on_device(): lax.all_to_all((expert_gate * gain_column[None]).astype(jnp.bfloat16), 'f...]
    psum x1 -> x0, waiting for transfers between devices: 11.4 us -> none  [on_device(): up_total = lax.psum(up_part.astype(jnp.bfloat16), 'tp').astype(jnp.float32)]
    dot_general x6 -> x0, matrix products: 6.82 us -> none  [the longest x1 2.18 us: on_device(): jnp.einsum('sch,dh->scd', hidden, served_down, preferred_element_type=jnp...]
    psum x1 -> x0, blocking collectives: 6.07 us -> none  [on_device(): lax.psum((jnp.sum(values, axis=1), jnp.sum(values * values, axis=1)), 'tp')]
    unnamed x27 -> x0, local copies, waits for them, and re-layouts: 5.34 us -> none
  transfers between devices with their start and end apart: 12 -> 0, of which waited for: 8 -> 0; matrix products, arithmetic and copies ran while one was open for 11% -> 0% of each run, Pallas kernels for 0% -> 0%
where the time goes in v2:
time: 62.2 us; the launch traced here: 61.7 us
  Pallas kernels  61.1 us (98%)
  between operations  0.64 us (1%)
    pallas_call x1, Pallas kernels, fused(): pl.pallas_call(functools.partial(fused_kernel, G, F, T, D, H), out_shape=...  58.5 us
    pallas_call x1, Pallas kernels, fused(): pl.pallas_call(write_kernel, out_shape=shapes, in_specs=[vm] * 7, out_spe...  2.61 us

profile of v2, /device:TPU:0, one launch (start us, length us, event | category | flops | bytes accessed | tf_op | source)
XLA Modules:
  0.0 61.7 jit_solution(4744413296568757999)
XLA Ops:
  0.6 58.5 %shard_map.153 = (bf16[512,256]{1,0:T(8,128)(2,1)}, bf16[512,256]{1,0:T(8,128)(2,1)}, bf16[512,256]{1,0:T(8,128)(2,1)}, bf16[512,256]{1,0:T(8,128)(2,1)}, bf16[5...) custom-call(bf16[128,512]{1,0:T(8,128)(2,1)} %tok.1, s32[2,128]{1,0:T(2,128)} %bitcast.19, ...), custom_call_target="tpu_custom_call" | custom-call | tf_op jit(solution)/shard_map/pallas_call | solution.py:389
  59.1 2.6 %shard_map.154 = (bf16[512,256]{1,0:T(8,128)(2,1)}, bf16[512,256]{1,0:T(8,128)(2,1)}, bf16[512,256]{1,0:T(8,128)(2,1)}, bf16[512,256]{1,0:T(8,128)(2,1)}, bf16[5...) custom-call(bf16[512,256]{1,0:T(8,128)(2,1)} %get-tuple-element.21.refs_0_, ...), custom_call_target="tpu_custom_call" | custom-call | tf_op jit(solution)/shard_map/pallas_call | solution.py:423

commit v3 on v2

--- a/solution.py
+++ b/solution.py
@@ -131,16 +131,16 @@
 
 def fused_kernel(
     G, F, T, D, H,
-    tok, routes, scores, gain, eg, eu, ed, sg, su, sd,
+    tok_in, routes, scores, gain, eg, eu, ed, sg, su, sd,
     o_sg, o_su, o_sd, o_cg, o_cu, o_cd, o_mix,
-    w32, sendg, sendd, sends, zg, zd, zs, we, de, ws,
+    tok, w32, sendg, sendd, sendc, sendf, zg, zd, zc, zf, we, de, wc, df,
     stat, tbuf, pbuf, rbuf, hbuf, obuf, ret,
-    l_sem, zg_s, zg_r, zd_s, zd_r, zs_s, zs_r, xg_s, xg_r, xd_s, xd_r, xs_s, xs_r,
+    l_sem, zg_s, zg_r, zd_s, zd_r, zc_s, zc_r, zf_s, zf_r, xg_s, xg_r, xd_s, xd_r, xc_s, xc_r, xf_s, xf_r,
     st_s, st_r, tk_s, tk_r, rs_s, rs_r, ag_s, ag_r, rt_s, rt_r,
 ):
     y, z, t = lax.axis_index("grp"), lax.axis_index("fs"), lax.axis_index("tp")
     E, Hs, Dz = eg.shape
-    R, FD = tok.shape
+    R, FD = tok_in.shape
     hr = Dz // G
     sr = R // T
     bf, f32 = jnp.bfloat16, jnp.float32
@@ -153,15 +153,6 @@
             src_ref=src, dst_ref=dst, send_sem=ss, recv_sem=rs,
             device_id=dev, device_id_type=pl.DeviceIdType.MESH,
         )
-
-    half = pl.ds(pl.multiple_of(y * hr, hr), hr)
-    loads = []
-    for i, (ref, sref) in enumerate(((eg, sg), (eu, su), (ed, sd))):
-        loads.append(pltpu.make_async_copy(ref.at[:, :, half], w32.at[i, pl.ds(0, E)], l_sem.at[2 * i]))
-        loads.append(pltpu.make_async_copy(sref.at[:, half], w32.at[i, E], l_sem.at[2 * i + 1]))
-    loads = [loads[0], loads[2], loads[4], loads[1], loads[3], loads[5]]
-    for c in loads:
-        c.start()
 
     barrier = pltpu.get_barrier_semaphore()
     peers = [at(y, lax.rem(z + d, F), t) for d in range(1, F)]
@@ -172,6 +163,18 @@
     for dev in peers:
         pl.semaphore_signal(barrier, inc=1, device_id=dev, device_id_type=pl.DeviceIdType.MESH)
 
+    half = pl.ds(pl.multiple_of(y * hr, hr), hr)
+    tok_load = pltpu.make_async_copy(tok_in, tok, l_sem.at[6])
+    tok_load.start()
+    loads = []
+    for i, (ref, sref) in enumerate(((eg, sg), (eu, su), (ed, sd))):
+        loads.append(pltpu.make_async_copy(ref.at[:, :, half], w32.at[i, pl.ds(0, E)], l_sem.at[2 * i]))
+        loads.append(pltpu.make_async_copy(sref.at[:, half], w32.at[i, E], l_sem.at[2 * i + 1]))
+    loads = [loads[0], loads[2], loads[4], loads[1], loads[3], loads[5]]
+    for c in loads:
+        c.start()
+
+    tok_load.wait()
     x = tok[...].astype(f32)
     s1 = jnp.sum(x, axis=1, keepdims=True)
     s2 = jnp.sum(x * x, axis=1, keepdims=True)
@@ -201,6 +204,11 @@
         pltpu.make_async_copy(src_of(z), zb.at[z], rr.at[z]).start()
 
     spread(lambda e: sendg.at[e], zg, zg_s, zg_r)
+
+    loads[2].wait()
+    for e in range(E):
+        sendd[e] = w32[2, e].astype(bf)
+    spread(lambda e: sendd.at[e], zd, zd_s, zd_r)
 
     for d in range(1, T):
         t2 = lax.rem(t + d, T)
@@ -217,15 +225,11 @@
         c.start()
         sent.append(c)
 
-    for c in loads[2:]:
+    for c in loads[3:]:
         c.wait()
-    for e in range(E):
-        sendd[e] = w32[2, e].astype(bf)
-    spread(lambda e: sendd.at[e], zd, zd_s, zd_r)
-    sends[0] = (w32[0, E] * gain_row).astype(bf)
-    sends[1] = (w32[1, E] * gain_row).astype(bf)
-    sends[2] = w32[2, E].astype(bf)
-    spread(lambda e: sends, zs, zs_s, zs_r)
+    sendc[0] = (w32[0, E] * gain_row).astype(bf)
+    sendc[1] = (w32[1, E] * gain_row).astype(bf)
+    sendf[...] = w32[2, E].astype(bf)
 
     held = []
 
@@ -261,8 +265,11 @@
     def at_d(ys, tt):
         return de.at[tt, :, columns(ys)]
 
-    def at_s(ys, tt):
-        return ws.at[:, tt, :, columns(ys)]
+    def at_c(ys, tt):
+        return wc.at[:, tt, :, columns(ys)]
+
+    def at_f(ys, tt):
+        return df.at[tt, :, columns(ys)]
 
     def rows_of(i):
         return pl.ds(pl.multiple_of(i * sr, sr), sr)
@@ -273,7 +280,7 @@
             pltpu.make_async_copy(tbuf.at[j], tbuf.at[j], tk_r.at[j]).wait()
         else:
             j = z
-        w = we[...] if s < F else ws[0:2]
+        w = we[...] if s < F else wc[...]
         pbuf[s] = (
             lax.dot_general(
                 tbuf[j], w.reshape(2 * H, FD), (((1,), (1,)), ((), ())), preferred_element_type=f32
@@ -304,7 +311,7 @@
             t2 = lax.rem(t + d, T)
             theirs = hbuf.at[s, rows_of(t2)]
             pltpu.make_async_copy(theirs, theirs, ag_r.at[s * T + t2]).wait()
-        w = de[...] if s < F else ws[2]
+        w = de[...] if s < F else df[...]
         value = jnp.dot(hbuf[s], w.reshape(H, FD), preferred_element_type=f32) * H ** (-0.5)
         if s == F:
             return value
@@ -319,25 +326,30 @@
     forward(zg, at_e, zg_r, xg_s, xg_r)
     arrived(at_e, xg_r)
     first(0)
-    for s in range(1, F):
+    forward(zd, at_d, zd_r, xd_s, xd_r)
+    first(1)
+    second(0)
+    arrived(at_d, xd_r)
+    second(1)
+    third(0)
+    for s in range(2, F):
         first(s)
-        second(s - 1)
-    second(F - 1)
-    forward(zd, at_d, zd_r, xd_s, xd_r)
-    arrived(at_d, xd_r)
-    for s in range(F):
-        third(s)
+        third(s - 1)
+        if s == 2:
+            spread(lambda e: sendc, zc, zc_s, zc_r)
+        second(s)
+    third(F - 1)
+    spread(lambda e: sendf, zf, zf_s, zf_r)
     o_sg[...] = we[0].reshape(H, FD).T
     o_su[...] = we[1].reshape(H, FD).T
     o_sd[...] = de[...].reshape(H, FD).T
-    forward(zs, at_s, zs_r, xs_s, xs_r)
-    arrived(at_s, xs_r)
+    forward(zc, at_c, zc_r, xc_s, xc_r)
+    arrived(at_c, xc_r)
     first(F)
-    o_cg[...] = ws[0].reshape(H, FD).T
+    o_cg[...] = wc[0].reshape(H, FD).T
     second(F)
-    o_cu[...] = ws[1].reshape(H, FD).T
-    o_cd[...] = ws[2].reshape(H, FD).T
-
+    o_cu[...] = wc[1].reshape(H, FD).T
+    forward(zf, at_f, zf_r, xf_s, xf_r)
     weight = scores[...] / jnp.sum(scores[...], axis=0, keepdims=True) * ROUTED_SCALE
     picked = routes[...]
     line = lax.broadcasted_iota(jnp.int32, (LANES, R), 0)
@@ -346,7 +358,9 @@
         share = jnp.sum(jnp.where(picked == e, weight, 0.0), axis=0, keepdims=True)
         shares = jnp.where(line == e, share, shares)
     shares = shares.T
+    arrived(at_f, xf_r)
     total = third(F)
+    o_cd[...] = df[...].reshape(H, FD).T
     for d in range(1, F):
         z2 = lax.rem(z + d, F)
         pltpu.make_async_copy(ret.at[z2], ret.at[z2], rt_r.at[z2]).wait()
@@ -358,16 +372,6 @@
         c.wait_send()
     for other, c in held:
         pl.when(other)(c.wait_send)
-
-
-def write_kernel(*refs):
-    count = (len(refs) - 1) // 2
-    sems = refs[-1]
-    copies = [pltpu.make_async_copy(refs[i], refs[count + i], sems.at[i]) for i in range(count)]
-    for c in copies:
-        c.start()
-    for c in copies:
-        c.wait()
 
 
 def fused(
@@ -388,20 +392,24 @@
     shapes = [weights] * 6 + [jax.ShapeDtypeStruct((R, FD), bf)]
     res = pl.pallas_call(
         functools.partial(fused_kernel, G, F, T, D, H),
-        out_shape=shapes,
-        in_specs=[vm] * 4 + [hbm] * 6,
+        out_shape=[pltpu.VMEM(s.shape, s.dtype) for s in shapes],
+        in_specs=[hbm] + [vm] * 3 + [hbm] * 6,
         out_specs=[vm] * 7,
         scratch_shapes=[
+            pltpu.VMEM((R, FD), bf),
             pltpu.VMEM((3, E + 1, Hs, hr), f32),
             pltpu.VMEM((E, 2, Hs, hr), bf),
             pltpu.VMEM((E, Hs, hr), bf),
-            pltpu.VMEM((3, Hs, hr), bf),
+            pltpu.VMEM((2, Hs, hr), bf),
+            pltpu.VMEM((Hs, hr), bf),
             pltpu.VMEM((F, 2, Hs, hr), bf),
             pltpu.VMEM((F, Hs, hr), bf),
-            pltpu.VMEM((F, 3, Hs, hr), bf),
+            pltpu.VMEM((F, 2, Hs, hr), bf),
+            pltpu.VMEM((F, Hs, hr), bf),
             pltpu.VMEM((2, T, Hs, FD), bf),
             pltpu.VMEM((T, Hs, FD), bf),
-            pltpu.VMEM((3, T, Hs, FD), bf),
+            pltpu.VMEM((2, T, Hs, FD), bf),
+            pltpu.VMEM((T, Hs, FD), bf),
             pltpu.VMEM((T, 8, R), f32),
             pltpu.VMEM((F, R, FD), bf),
             pltpu.VMEM((B, R, 2 * H), bf),
@@ -409,8 +417,8 @@
             pltpu.VMEM((B, R, H), bf),
             pltpu.VMEM((F, R, FD), bf),
             pltpu.VMEM((F, R, FD), bf),
-            dma(6), dma(F), dma(F), dma(F), dma(F), dma(F), dma(F),
-            dma(F * G), dma(G * T), dma(F * G), dma(G * T), dma(F * G), dma(G * T),
+            dma(7), dma(F), dma(F), dma(F), dma(F), dma(F), dma(F), dma(F), dma(F),
+            dma(F * G), dma(G * T), dma(F * G), dma(G * T), dma(F * G), dma(G * T), dma(F * G), dma(G * T),
             dma(T), dma(T), dma(F), dma(F),
             dma(B * T), dma(B * T), dma(B * T), dma(B * T), dma(F), dma(F),
         ],
@@ -420,13 +428,6 @@
         jnp.swapaxes(expert_gate, 1, 2), jnp.swapaxes(expert_up, 1, 2), jnp.swapaxes(expert_down, 1, 2),
         shared_gate.T, shared_up.T, shared_down.T,
     )
-    res = pl.pallas_call(
-        write_kernel,
-        out_shape=shapes,
-        in_specs=[vm] * 7,
-        out_specs=[hbm] * 7,
-        scratch_shapes=[dma(7)],
-    )(*res)
     return tuple(r[None] for r in res[:3]) + tuple(res[3:])
 
 

time: 62.2 us -> 68.9 us (1.11)
  local copies, waits for them, and re-layouts: 0 us -> 4.87 us
  Pallas kernels: 61.1 us -> 63 us
    unnamed x0 -> x7, local copies, waits for them, and re-layouts: none -> 4.87 us
    pallas_call x1, Pallas kernels: 58.5 us -> 63 us  [fused(): pl.pallas_call(functools.partial(fused_kernel, G, F, T, D, H), out_shape=...]
    pallas_call x1 -> x0, Pallas kernels: 2.61 us -> none  [fused(): pl.pallas_call(write_kernel, out_shape=shapes, in_specs=[vm] * 7, out_spe...]
where the time goes in v3:
time: 68.9 us; the launch traced here: 68.5 us
  Pallas kernels  63 us (91%)
  local copies, waits for them, and re-layouts  4.87 us (7%)
    pallas_call x1, Pallas kernels, fused(): pl.pallas_call(functools.partial(fused_kernel, G, F, T, D, H), out_shape=...  63 us
    unnamed x7, local copies, waits for them, and re-layouts  4.87 us

profile of v3, /device:TPU:0, one launch (start us, length us, event | category | flops | bytes accessed | tf_op | source)
XLA Modules:
  0.0 68.5 jit_solution(724524458363025854)
XLA Ops:
  0.6 63.0 %shard_map.153 = (bf16[512,256]{1,0:T(8,128)(2,1)S(1)}, bf16[512,256]{1,0:T(8,128)(2,1)S(1)}, bf16[512,256]{1,0:T(8,128)(2,1)S(1)}, bf16[512,256]{1,0:T(8,128)(2...) custom-call(bf16[128,512]{1,0:T(8,128)(2,1)} %tok_in.1, ...), custom_call_target="tpu_custom_call" | custom-call | tf_op jit(solution)/shard_map/pallas_call | solution.py:393
  63.7 0.7 %copy.24 = bf16[1,512,256]{2,1,0:T(8,128)(2,1)} copy(bf16[1,512,256]{2,1,0:T(8,128)(2,1)S(1)} %bitcast.14) | data formatting | bytes 524288
  64.4 0.7 %copy.25 = bf16[1,512,256]{2,1,0:T(8,128)(2,1)} copy(bf16[1,512,256]{2,1,0:T(8,128)(2,1)S(1)} %bitcast.13) | data formatting | bytes 524288
  65.1 0.7 copy.30
  65.7 0.7 %copy.26 = bf16[1,512,256]{2,1,0:T(8,128)(2,1)} copy(bf16[1,512,256]{2,1,0:T(8,128)(2,1)S(1)} %bitcast.12) | data formatting | bytes 524288
  66.4 0.7 %copy.27 = bf16[512,256]{1,0:T(8,128)(2,1)} copy(bf16[512,256]{1,0:T(8,128)(2,1)S(1)} %get-tuple-element.24) | data formatting | bytes 524288
  67.1 0.7 %copy.28 = bf16[512,256]{1,0:T(8,128)(2,1)} copy(bf16[512,256]{1,0:T(8,128)(2,1)S(1)} %get-tuple-element.25) | data formatting | bytes 524288
  67.8 0.7 %copy.29 = bf16[512,256]{1,0:T(8,128)(2,1)} copy(bf16[512,256]{1,0:T(8,128)(2,1)S(1)} %get-tuple-element.26) | data formatting | bytes 524288
